TPU v7x, 32 devices: a whole 2x2x4 slice. The times are simulated.
32 devices in a mesh: grp: 2 (over y), fs: 4 (over z), tp: 4 (over x, core).
Axes of the slice: x: 2, y: 2, z: 4, core: 2. Of those that a mesh axis runs over, the one named last changes fastest.
Arguments:
- tokens: bfloat16 [2560, 2048], P(('grp', 'fs', 'tp')), parts along dimension 0, may hold values from -6 to 6
- mix_gain: bfloat16 [2048], replicated, may hold values from 0.099609375 to 1.8984375
- val_weight: bfloat16 [2048, 1024], P('fs', 'tp'), may hold values from -4 to 4
- gate_weight: bfloat16 [2048, 1024], P('fs', 'tp'), may hold values from -0.125 to 0.125
- conv_taps: bfloat16 [31, 1024], replicated, may hold values from -1 to 1
- chan_gain: bfloat16 [1024], replicated, may hold values from 0.099609375 to 1.8984375
- out_weight: bfloat16 [1024, 2048], P('tp', 'fs'), may hold values from -0.1875 to 0.1875
- mix_post_gain: bfloat16 [2048], replicated, may hold values from 0.099609375 to 1.8984375
- ffn_gain: bfloat16 [2048], replicated, may hold values from 0.099609375 to 1.8984375
- up_gate_weight: bfloat16 [2048, 5120], P('fs', 'tp'), may hold values from -0.125 to 0.125
- up_val_weight: bfloat16 [2048, 5120], P('fs', 'tp'), may hold values from -0.125 to 0.125
- ffn_taps: bfloat16 [2, 3, 5120], replicated, may hold values from -3.5 to 3.5
- down_weight: bfloat16 [5120, 2048], P('tp', 'fs'), may hold values from -0.078125 to 0.078125
- ffn_post_gain: bfloat16 [2048], replicated, may hold values from 0.099609375 to 1.8984375
Outputs:
- layer_out: bfloat16 [2560, 2048], P(('grp', 'fs', 'tp')), parts along dimension 0
There are 2 independent parts, one for each index of `grp`. A program takes and returns all parts, laid end to end along the dimension named above; an argument that names none is the same for every part. Nothing has to cross between parts.
All inputs are finite; a program needn't handle non-finite values.
Results may differ from a plain program's by a relative error of at most 0.019.
Values may be sent and summed in bfloat16 or wider, within the bound.
A program may use at most 64 MiB of HBM per device.

v0:
```python
import jax
import jax.numpy as jnp
from jax import lax
from jax.sharding import PartitionSpec as P

LEN = 64
norm_epsilon = 1e-06
chan_epsilon = 1e-05


def rms_scale(values, gain):
    inverse = lax.rsqrt(jnp.mean(values * values, axis=-1, keepdims=True) + norm_epsilon)
    return values * inverse * gain.astype(jnp.float32)


def depthwise(signal, tap_table):
    taps_count = tap_table.shape[0]
    channels = signal.shape[1]
    shaped = signal.astype(jnp.float32).reshape(signal.shape[0] // LEN, LEN, channels)
    padded = jnp.pad(shaped, ((0, 0), (taps_count - 1, 0), (0, 0)))
    tap_values = tap_table.astype(jnp.float32)
    result = jnp.zeros(shaped.shape, jnp.float32)
    for offset in range(taps_count):
        result = result + padded[:, offset : offset + LEN, :] * tap_values[offset]
    return result.reshape(signal.shape[0], channels)


def make_adder(left, pieces):
    first = jnp.dot(left, pieces[0], preferred_element_type=jnp.float32)
    second = jnp.dot(left, pieces[1], preferred_element_type=jnp.float32)
    return (first, second)


def make_rows_product(left, weight):
    return jnp.dot(left, weight, preferred_element_type=jnp.float32)


def shards(
    tokens,
    mix_gain,
    val_weight,
    gate_weight,
    conv_taps,
    chan_gain,
    out_weight,
    mix_post_gain,
    ffn_gain,
    up_gate_weight,
    up_val_weight,
    ffn_taps,
    down_weight,
    ffn_post_gain,
):
    member = lax.axis_index("tp")
    normed_own = rms_scale(tokens.astype(jnp.float32), mix_gain).astype(jnp.bfloat16)
    normed = lax.all_gather(normed_own, "tp", axis=0, tiled=True)
    local_ch = val_weight.shape[1]
    values, gate_sums = make_adder(
        normed,
        (
            lax.all_gather(val_weight, "fs", axis=0, tiled=True),
            lax.all_gather(gate_weight, "fs", axis=0, tiled=True),
        ),
    )
    glu_out = (values * jax.nn.sigmoid(gate_sums)).astype(jnp.bfloat16)
    own_taps = lax.dynamic_slice_in_dim(conv_taps, member * local_ch, local_ch, 1)
    conv_out = depthwise(glu_out, own_taps)
    totals, squares = lax.psum(
        (jnp.sum(conv_out, axis=1), jnp.sum(conv_out * conv_out, axis=1)), "tp"
    )
    all_channels = chan_gain.shape[0]
    chan_mean = totals[:, None] / all_channels
    chan_var = squares[:, None] / all_channels - chan_mean * chan_mean
    own_gain = lax.dynamic_slice_in_dim(chan_gain, member * local_ch, local_ch, 0).astype(
        jnp.float32
    )
    activated = jax.nn.silu((conv_out - chan_mean) * lax.rsqrt(chan_var + chan_epsilon) * own_gain)
    activated = activated.astype(jnp.bfloat16)
    out_full = lax.all_gather(out_weight, "fs", axis=1, tiled=True)
    mixed_sum = lax.psum_scatter(
        make_rows_product(activated, out_full).astype(jnp.bfloat16),
        "tp",
        scatter_dimension=0,
        tiled=True,
    ).astype(jnp.float32)
    residual = (tokens.astype(jnp.float32) + rms_scale(mixed_sum, mix_post_gain)).astype(
        jnp.bfloat16
    )
    normed_share = rms_scale(residual.astype(jnp.float32), ffn_gain).astype(jnp.bfloat16)
    normed_ffn = lax.all_gather(normed_share, "tp", axis=0, tiled=True)
    local_ff = up_gate_weight.shape[1]
    own_ffn_taps = lax.dynamic_slice_in_dim(ffn_taps, member * local_ff, local_ff, 2)
    gate_full, val_full = (
        lax.all_gather(up_gate_weight, "fs", axis=0, tiled=True),
        lax.all_gather(up_val_weight, "fs", axis=0, tiled=True),
    )
    up_gate = jnp.dot(normed_ffn, gate_full, preferred_element_type=jnp.float32).astype(
        jnp.bfloat16
    )
    up_val = jnp.dot(normed_ffn, val_full, preferred_element_type=jnp.float32).astype(jnp.bfloat16)
    gate_conv = depthwise(up_gate, own_ffn_taps[0])
    val_conv = depthwise(up_val, own_ffn_taps[1])
    hidden = (jax.nn.gelu(gate_conv, approximate=True) * val_conv).astype(jnp.bfloat16)
    down_full = lax.all_gather(down_weight, "fs", axis=1, tiled=True)
    ffn_sum = lax.psum_scatter(
        make_rows_product(hidden, down_full).astype(jnp.bfloat16),
        "tp",
        scatter_dimension=0,
        tiled=True,
    ).astype(jnp.float32)
    return (residual.astype(jnp.float32) + rms_scale(ffn_sum, ffn_post_gain)).astype(jnp.bfloat16)


def solution(mesh):
    return jax.shard_map(
        shards,
        mesh=mesh,
        in_specs=(
            P(("grp", "fs", "tp"), None),
            P(),
            P("fs", "tp"),
            P("fs", "tp"),
            P(),
            P(),
            P("tp", "fs"),
            P(),
            P(),
            P("fs", "tp"),
            P("fs", "tp"),
            P(),
            P("tp", "fs"),
            P(),
        ),
        out_specs=P(("grp", "fs", "tp"), None),
        check_vma=False,
    )
```

profile of v0, /device:TPU:0, one launch (start us, length us, event | category | flops | bytes accessed | tf_op | source)
XLA Modules:
  0.0 503.6 jit_solution(17224619364062690328)
XLA Ops:
  8.0 1.1 fusion.26
  9.1 1.8 fusion.28
  13.9 25.7 %all-gather.11.cloned.1.call-done = bf16[2048,256]{1,0:T(8,128)(2,1)} async-done(((bf16[512,256]{1,0:T(8,128)(2,1)}), bf16[2048,256]{1,0:T(8,128)(2,1)}) %all-gather.11.cloned.1.call-update) | async-done | bytes 1048592 | tf_op jit(solution)/shard_map/all_gather | solution.py:61
  39.7 19.1 %all-gather.9.cloned.1.call-done = bf16[320,2048]{1,0:T(8,128)(2,1)} async-done(((bf16[80,2048]{1,0:T(8,128)(2,1)}), bf16[320,2048]{1,0:T(8,128)(2,1)}) %all-gather.9.cloned.1.call-update) | async-done | bytes 1310736 | tf_op jit(solution)/shard_map/all_gather | solution.py:56
  58.8 2.2 fusion.101
  61.0 27.4 %all-gather.13.cloned.1.call-done = bf16[2048,256]{1,0:T(8,128)(2,1)} async-done(((bf16[512,256]{1,0:T(8,128)(2,1)}), bf16[2048,256]{1,0:T(8,128)(2,1)}) %all-gather.13.cloned.1.call-update) | async-done | bytes 1048592 | tf_op jit(solution)/shard_map/all_gather | solution.py:62
  88.4 1.7 fusion.21
  90.2 1.2 fusion.96
  91.5 6.1 %all-reduce.3 = (f32[320]{0:T(512)S(1)}, f32[320]{0:T(512)S(1)}) all-reduce(f32[320]{0:T(512)S(1)} %reduce_sum.62, f32[320]{0:T(512)S(1)} %reduce_sum.60), channel_id=1, replica_groups=mesh['grp'=2,'fs'=4,'tp'=4] {'tp'}, use_global_device_ids=true, to_apply=%region_4.5 | all-reduce | flops 640 | bytes 5120 | tf_op jit(solution)/shard_map/psum | solution.py:68
  97.8 19.4 %all-gather.15.cloned.1.call-done = bf16[256,2048]{1,0:T(8,128)(2,1)} async-done(((bf16[256,512]{1,0:T(8,128)(2,1)}), bf16[256,2048]{1,0:T(8,128)(2,1)}) %all-gather.15.cloned.1.call-update) | async-done | bytes 1048592 | tf_op jit(solution)/shard_map/all_gather | solution.py:79
  117.2 2.8 convolution_convert_fusion.3
  120.1 25.9 %reduce-scatter.3.cloned.1.call-done = bf16[80,2048]{1,0:T(8,128)(2,1)} async-done(((bf16[320,2048]{1,0:T(8,128)(2,1)}), bf16[80,2048]{1,0:T(8,128)(2,1)}) %reduce-scatter.3.cloned.1.call-update) | async-done | bytes 327696 | tf_op jit(solution)/shard_map/reduce_scatter | solution.py:80
  146.0 1.1 fusion.22
  147.1 1.3 fusion.30
  151.9 15.8 %all-gather.17.cloned.1.call-done = bf16[320,2048]{1,0:T(8,128)(2,1)} async-done(((bf16[80,2048]{1,0:T(8,128)(2,1)}), bf16[320,2048]{1,0:T(8,128)(2,1)}) %all-gather.17.cloned.1.call-update) | async-done | bytes 1310736 | tf_op jit(solution)/shard_map/all_gather | solution.py:90
  167.7 99.6 %all-gather.19.cloned.1.call-done = bf16[2048,1280]{1,0:T(8,128)(2,1)} async-done(((bf16[512,1280]{1,0:T(8,128)(2,1)}), bf16[2048,1280]{1,0:T(8,128)(2,1)}) %all-gather.19.cloned.1.call-update) | async-done | bytes 5242896 | tf_op jit(solution)/shard_map/all_gather | solution.py:94
  267.3 4.8 convolution_convert_fusion.2
  272.2 93.1 %all-gather.21.cloned.1.call-done = bf16[2048,1280]{1,0:T(8,128)(2,1)} async-done(((bf16[512,1280]{1,0:T(8,128)(2,1)}), bf16[2048,1280]{1,0:T(8,128)(2,1)}) %all-gather.21.cloned.1.call-update) | async-done | bytes 5242896 | tf_op jit(solution)/shard_map/all_gather | solution.py:95
  365.3 4.3 convolution_convert_fusion.1
  371.3 92.0 %all-gather.23.cloned.1.call-done = bf16[1280,2048]{1,0:T(8,128)(2,1)} async-done(((bf16[1280,512]{1,0:T(8,128)(2,1)}), bf16[1280,2048]{1,0:T(8,128)(2,1)}) %all-gather.23.cloned.1.call-update) | async-done | bytes 5242896 | tf_op jit(solution)/shard_map/all_gather | solution.py:104
  463.3 5.5 %convolution_convert_fusion = bf16[320,2048]{1,0:T(8,128)(2,1)} fusion(bf16[320,1280]{1,0:T(8,128)(2,1)S(1)} %fusion.16, bf16[1280,2048]{1,0:T(8,128)(2,1)} %all-gather.23.cloned.1.call-done), kind=kOutput, calls=%fused_computation | convolution fusion | flops 1678376960 | bytes 7372800 | tf_op jit(solution)/shard_map/dot_general | solution.py:35
  468.8 24.9 %reduce-scatter.5.cloned.1.call-done = bf16[80,2048]{1,0:T(8,128)(2,1)} async-done(((bf16[320,2048]{1,0:T(8,128)(2,1)}), bf16[80,2048]{1,0:T(8,128)(2,1)}) %reduce-scatter.5.cloned.1.call-update) | async-done | bytes 327696 | tf_op jit(solution)/shard_map/reduce_scatter | solution.py:105
  493.7 1.1 fusion.24
  494.9 1.9 fusion.33
  (59 shorter events, 9.9 us)
Async XLA Ops:
  6.5 33.1 %all-gather.11.cloned.1.call-start = ((), (), s32[]{:S(2)}) async-start(), calls=%async_computation.3 | async-start | bytes 1310720 | tf_op jit(solution)/shard_map/all_gather | solution.py:61
  7.3 51.5 %all-gather.9.cloned.1.call-start = ((), (), s32[]{:S(2)}) async-start(), calls=%async_computation.2 | async-start | bytes 1638400 | tf_op jit(solution)/shard_map/all_gather | solution.py:56
  11.0 77.4 %all-gather.13.cloned.1.call-start = ((), (), s32[]{:S(2)}) async-start(), calls=%async_computation.4 | async-start | bytes 1310720 | tf_op jit(solution)/shard_map/all_gather | solution.py:62
  11.8 105.4 %all-gather.15.cloned.1.call-start = ((), (), s32[]{:S(2)}) async-start(), calls=%async_computation.5 | async-start | bytes 1310720 | tf_op jit(solution)/shard_map/all_gather | solution.py:79
  12.3 133.6 %reduce-scatter.3.cloned.1.call-start = ((), (), s32[]{:S(2)}) async-start(), calls=%async_computation.6 | async-start | bytes 1638400 | tf_op jit(solution)/shard_map/reduce_scatter | solution.py:80
  58.8 29.6 %copy-start.5 = (bf16[320,2048]{1,0:T(8,128)(2,1)S(1)}, bf16[320,2048]{1,0:T(8,128)(2,1)}, u32[]{:S(2)}) copy-start(bf16[320,2048]{1,0:T(8,128)(2,1)} %all-gather.9.cloned.1.call-done) | copy-start | bytes 3932164
  97.8 22.3 %copy-start.2 = (bf16[2048]{0:T(1024)(128)(2,1)S(1)}, bf16[2048]{0:T(1024)(128)(2,1)}, u32[]{:S(2)}) copy-start(bf16[2048]{0:T(1024)(128)(2,1)} %param.21) | copy-start | bytes 12292
  97.8 22.3 %copy-start.3 = (bf16[2048]{0:T(1024)(128)(2,1)S(1)}, bf16[2048]{0:T(1024)(128)(2,1)}, u32[]{:S(2)}) copy-start(bf16[2048]{0:T(1024)(128)(2,1)} %param.22) | copy-start | bytes 12292
  97.8 49.3 %copy-start = (bf16[80,2048]{1,0:T(8,128)(2,1)S(1)}, bf16[80,2048]{1,0:T(8,128)(2,1)}, u32[]{:S(2)}) copy-start(bf16[80,2048]{1,0:T(8,128)(2,1)} %param.14) | copy-start | bytes 983044
  120.0 47.7 %all-gather.17.cloned.1.call-start = ((), (), s32[]{:S(2)}) async-start(), calls=%async_computation.7 | async-start | bytes 1638400 | tf_op jit(solution)/shard_map/all_gather | solution.py:90
  149.4 118.0 %all-gather.19.cloned.1.call-start = ((), (), s32[]{:S(2)}) async-start(), calls=%async_computation.8 | async-start | bytes 6553600 | tf_op jit(solution)/shard_map/all_gather | solution.py:94
  150.1 1.5 copy-start.1
  150.1 215.2 %all-gather.21.cloned.1.call-start = ((), (), s32[]{:S(2)}) async-start(), calls=%async_computation.9 | async-start | bytes 6553600 | tf_op jit(solution)/shard_map/all_gather | solution.py:95
  150.9 312.4 %all-gather.23.cloned.1.call-start = ((), (), s32[]{:S(2)}) async-start(), calls=%async_computation.10 | async-start | bytes 6553600 | tf_op jit(solution)/shard_map/all_gather | solution.py:104
  151.6 342.1 %reduce-scatter.5.cloned.1.call-start = ((), (), s32[]{:S(2)}) async-start(), calls=%async_computation.11 | async-start | bytes 1638400 | tf_op jit(solution)/shard_map/reduce_scatter | solution.py:105
  272.1 93.2 %copy-start.6 = (bf16[320,2048]{1,0:T(8,128)(2,1)S(1)}, bf16[320,2048]{1,0:T(8,128)(2,1)}, u32[]{:S(2)}) copy-start(bf16[320,2048]{1,0:T(8,128)(2,1)} %all-gather.17.cloned.1.call-done) | copy-start | bytes 3932164
  371.3 97.5 %copy-start.4 = (bf16[2048]{0:T(1024)(128)(2,1)S(1)}, bf16[2048]{0:T(1024)(128)(2,1)}, u32[]{:S(2)}) copy-start(bf16[2048]{0:T(1024)(128)(2,1)} %param.27) | copy-start | bytes 12292
Sparse Core Ops, SparseCore 0:
  8.9 30.7 all-gather.10
  41.2 17.5 all-gather.8
  60.4 27.9 all-gather.12
  89.8 27.3 all-gather.14
  120.1 25.7 reduce-scatter.2
  149.5 18.1 all-gather.16
  169.3 98.0 all-gather.18
  268.9 96.3 all-gather.20
  366.9 96.3 all-gather.22
  468.9 24.7 reduce-scatter.4
where the time goes:
time: 504 us
  waiting for transfers between devices  447 us (89%)
  matrix products  21.4 us (4%)
  other arithmetic  14.9 us (3%)
  between operations  13.8 us (3%)
  blocking collectives  6.05 us (1%)
    all_gather x1, waiting for transfers between devices, shards(): lax.all_gather(up_gate_weight, 'fs', axis=0, tiled=True)  99.6 us
    all_gather x1, waiting for transfers between devices, shards(): lax.all_gather(up_val_weight, 'fs', axis=0, tiled=True)  93.1 us
    all_gather x1, waiting for transfers between devices, shards(): down_full = lax.all_gather(down_weight, 'fs', axis=1, tiled=True)  92 us
    all_gather x1, waiting for transfers between devices, shards(): lax.all_gather(gate_weight, 'fs', axis=0, tiled=True)  27.4 us
    reduce_scatter x1, waiting for transfers between devices, shards(): lax.psum_scatter(make_rows_product(activated, out_full).astype(jnp.bfloat...  25.9 us
    all_gather x1, waiting for transfers between devices, shards(): lax.all_gather(val_weight, 'fs', axis=0, tiled=True)  25.7 us
    reduce_scatter x1, waiting for transfers between devices, shards(): lax.psum_scatter(make_rows_product(hidden, down_full).astype(jnp.bfloat16...  24.9 us
    all_gather x1, waiting for transfers between devices, shards(): out_full = lax.all_gather(out_weight, 'fs', axis=1, tiled=True)  19.4 us
  transfers between devices with their start and end apart: 10, of which 10 were waited for; matrix products, arithmetic and copies ran while one was open for 4% of the time, Pallas kernels for 0%

commit v1 on v0

--- a/solution.py
+++ b/solution.py
@@ -6,6 +6,16 @@
 LEN = 64
 norm_epsilon = 1e-06
 chan_epsilon = 1e-05
+
+
+def pass_along(x, axis, along):
+    count = lax.axis_size(axis)
+    current, parts = (x, [x])
+    for _ in range(count - 1):
+        current = lax.ppermute(current, axis, [(i, (i + 1) % count) for i in range(count)])
+        parts.insert(0, current)
+    line = jnp.concatenate(parts, axis=along)
+    return jnp.roll(line, (lax.axis_index(axis) + 1) * x.shape[along], axis=along)
 
 
 def rms_scale(values, gain):
@@ -101,7 +111,7 @@
     gate_conv = depthwise(up_gate, own_ffn_taps[0])
     val_conv = depthwise(up_val, own_ffn_taps[1])
     hidden = (jax.nn.gelu(gate_conv, approximate=True) * val_conv).astype(jnp.bfloat16)
-    down_full = lax.all_gather(down_weight, "fs", axis=1, tiled=True)
+    down_full = pass_along(down_weight, "fs", 1)
     ffn_sum = lax.psum_scatter(
         make_rows_product(hidden, down_full).astype(jnp.bfloat16),
         "tp",

time: 504 us -> 463 us (0.919)
  waiting for transfers between devices: 447 us -> 355 us
  starting transfers between devices: 0.36 us -> 35.5 us
  local copies, waits for them, and re-layouts: 0.3 us -> 15.8 us
    ppermute x0 -> x3, waiting for transfers between devices: none -> 138 us  [pass_along(): lax.ppermute(current, axis, [(i, (i + 1) % count) for i in range(count)])]
    all_gather x1, waiting for transfers between devices: 99.6 us -> 0.01 us  [shards(): lax.all_gather(up_gate_weight, 'fs', axis=0, tiled=True)]
    all_gather x1 -> x0, waiting for transfers between devices: 92 us -> none  [shards(): down_full = lax.all_gather(down_weight, 'fs', axis=1, tiled=True)]
    ppermute x0 -> x3, starting transfers between devices: none -> 35.2 us  [pass_along(): lax.ppermute(current, axis, [(i, (i + 1) % count) for i in range(count)])]
    all_gather x1, waiting for transfers between devices: 93.1 us -> 71.8 us  [shards(): lax.all_gather(up_val_weight, 'fs', axis=0, tiled=True)]
    all_gather x1, waiting for transfers between devices: 15.8 us -> 0.01 us  [shards(): normed_ffn = lax.all_gather(normed_share, 'tp', axis=0, tiled=True)]
    unnamed x14 -> x21, local copies, waits for them, and re-layouts: 0.04 us -> 14.3 us
  transfers between devices with their start and end apart: 10 -> 12, of which waited for: 10 -> 10; matrix products, arithmetic and copies ran while one was open for 4% -> 7% of each run, Pallas kernels for 0% -> 0%
where the time goes in v1:
time: 463 us
  waiting for transfers between devices  355 us (77%)
  starting transfers between devices  35.5 us (8%)
  matrix products  21.8 us (5%)
  local copies, waits for them, and re-layouts  15.8 us (3%)
  other arithmetic  14.9 us (3%)
  between operations  13.5 us (3%)
  blocking collectives  6.05 us (1%)
    ppermute x3, waiting for transfers between devices, pass_along(): lax.ppermute(current, axis, [(i, (i + 1) % count) for i in range(count)])  138 us
    all_gather x1, waiting for transfers between devices, shards(): lax.all_gather(up_val_weight, 'fs', axis=0, tiled=True)  71.8 us
    ppermute x3, starting transfers between devices, pass_along(): lax.ppermute(current, axis, [(i, (i + 1) % count) for i in range(count)])  35.2 us
    all_gather x1, waiting for transfers between devices, shards(): lax.all_gather(gate_weight, 'fs', axis=0, tiled=True)  27.4 us
    reduce_scatter x1, waiting for transfers between devices, shards(): lax.psum_scatter(make_rows_product(activated, out_full).astype(jnp.bfloat...  25.9 us
    all_gather x1, waiting for transfers between devices, shards(): lax.all_gather(val_weight, 'fs', axis=0, tiled=True)  25.7 us
    reduce_scatter x1, waiting for transfers between devices, shards(): lax.psum_scatter(make_rows_product(hidden, down_full).astype(jnp.bfloat16...  24.9 us
    all_gather x1, waiting for transfers between devices, shards(): out_full = lax.all_gather(out_weight, 'fs', axis=1, tiled=True)  19.4 us
  transfers between devices with their start and end apart: 12, of which 10 were waited for; matrix products, arithmetic and copies ran while one was open for 7% of the time, Pallas kernels for 0%

profile of v1, /device:TPU:0, one launch (start us, length us, event | category | flops | bytes accessed | tf_op | source)
XLA Modules:
  0.0 462.6 jit_solution(6617423647172538523)
XLA Ops:
  9.1 1.8 fusion.33
  13.9 25.7 %all-gather.10.cloned.1.call-done = bf16[2048,256]{1,0:T(8,128)(2,1)} async-done(((bf16[512,256]{1,0:T(8,128)(2,1)}), bf16[2048,256]{1,0:T(8,128)(2,1)}) %all-gather.10.cloned.1.call-update) | async-done | bytes 1048592 | tf_op jit(solution)/shard_map/all_gather | solution.py:71
  39.7 19.1 %all-gather.8.cloned.1.call-done = bf16[320,2048]{1,0:T(8,128)(2,1)} async-done(((bf16[80,2048]{1,0:T(8,128)(2,1)}), bf16[320,2048]{1,0:T(8,128)(2,1)}) %all-gather.8.cloned.1.call-update) | async-done | bytes 1310736 | tf_op jit(solution)/shard_map/all_gather | solution.py:66
  58.8 2.2 fusion.107
  61.0 27.4 %all-gather.12.cloned.1.call-done = bf16[2048,256]{1,0:T(8,128)(2,1)} async-done(((bf16[512,256]{1,0:T(8,128)(2,1)}), bf16[2048,256]{1,0:T(8,128)(2,1)}) %all-gather.12.cloned.1.call-update) | async-done | bytes 1048592 | tf_op jit(solution)/shard_map/all_gather | solution.py:72
  91.5 6.0 %all-reduce.3 = (f32[320]{0:T(512)S(1)}, f32[320]{0:T(512)S(1)}) all-reduce(f32[320]{0:T(512)S(1)} %reduce_sum.62, f32[320]{0:T(512)S(1)} %reduce_sum.60), channel_id=1, replica_groups=mesh['grp'=2,'fs'=4,'tp'=4] {'tp'}, use_global_device_ids=true, to_apply=%region_4.5 | all-reduce | flops 640 | bytes 5120 | tf_op jit(solution)/shard_map/psum | solution.py:78
  97.8 19.4 %all-gather.14.cloned.1.call-done = bf16[256,2048]{1,0:T(8,128)(2,1)} async-done(((bf16[256,512]{1,0:T(8,128)(2,1)}), bf16[256,2048]{1,0:T(8,128)(2,1)}) %all-gather.14.cloned.1.call-update) | async-done | bytes 1048592 | tf_op jit(solution)/shard_map/all_gather | solution.py:89
  117.2 2.8 convolution_convert_fusion.2
  120.1 25.9 %reduce-scatter.3.cloned.1.call-done = bf16[80,2048]{1,0:T(8,128)(2,1)} async-done(((bf16[320,2048]{1,0:T(8,128)(2,1)}), bf16[80,2048]{1,0:T(8,128)(2,1)}) %reduce-scatter.3.cloned.1.call-update) | async-done | bytes 327696 | tf_op jit(solution)/shard_map/reduce_scatter | solution.py:90
  152.5 32.1 %collective-permute-done = bf16[1280,512]{1,0:T(8,128)(2,1)S(1)} collective-permute-done((bf16[1280,512]{1,0:T(8,128)(2,1)S(1)}, bf16[1280,512]{1,0:T(8,128)(2,1)S(1)}, u32[]{:S(2)}, u32[]{:S(2)}) %collective-permute-start) | collective-permute-done | bytes 1310752 | tf_op jit(solution)/shard_map/ppermute | solution.py:15
  184.6 4.5 collective-permute-start.1
  189.1 57.1 %collective-permute-done.1 = bf16[1280,512]{1,0:T(8,128)(2,1)} collective-permute-done((bf16[1280,512]{1,0:T(8,128)(2,1)S(1)}, bf16[1280,512]{1,0:T(8,128)(2,1)}, u32[]{:S(2)}, u32[]{:S(2)}) %collective-permute-start.1) | collective-permute-done | bytes 1310752 | tf_op jit(solution)/shard_map/ppermute | solution.py:15
  246.1 29.1 %collective-permute-start.2 = (bf16[1280,512]{1,0:T(8,128)(2,1)}, bf16[1280,512]{1,0:T(8,128)(2,1)}, u32[]{:S(2)}, u32[]{:S(2)}) collective-permute-start(bf16[1280,512]{1,0:T(8,128)(2,1)} %collective-permute-done.1), channel_id=1, source_target_pairs={{0,4},{4,8},{8,12},{12,0},{1,5},{5,9},{9,13},{13,1},{2,6},{6,10},{... | collective-permute-start | bytes 3932168 | tf_op jit(solution)/shard_map/ppermute | solution.py:15
  275.5 48.4 %collective-permute-done.2 = bf16[1280,512]{1,0:T(8,128)(2,1)} collective-permute-done((bf16[1280,512]{1,0:T(8,128)(2,1)}, bf16[1280,512]{1,0:T(8,128)(2,1)}, u32[]{:S(2)}, u32[]{:S(2)}) %collective-permute-start.2) | collective-permute-done | bytes 1310752 | tf_op jit(solution)/shard_map/ppermute | solution.py:15
  323.9 2.7 constant_dynamic-update-slice_fusion.7
  326.6 2.7 constant_dynamic-update-slice_fusion.6
  331.8 2.5 constant_dynamic-update-slice_fusion.3
  334.3 2.6 constant_dynamic-update-slice_fusion.2
  339.4 4.8 %convolution_convert_fusion.1 = bf16[320,1280]{1,0:T(8,128)(2,1)S(1)} fusion(bf16[320,2048]{1,0:T(8,128)(2,1)} %all-gather.16.cloned.1.call-done, bf16[2048,1280]{1,0:T(8,128)(2,1)} %all-gather.18.cloned.1.call-done), kind=kOutput, calls=%fused_computation.4 | convolution fusion | flops 1678131200 | bytes 7372800 | tf_op jit(solution)/shard_map/dot_general | solution.py:107
  344.4 71.8 %all-gather.20.cloned.1.call-done = bf16[2048,1280]{1,0:T(8,128)(2,1)} async-done(((bf16[512,1280]{1,0:T(8,128)(2,1)}), bf16[2048,1280]{1,0:T(8,128)(2,1)}) %all-gather.20.cloned.1.call-update) | async-done | bytes 5242896 | tf_op jit(solution)/shard_map/all_gather | solution.py:105
  416.2 4.7 %convolution_convert_fusion = bf16[320,1280]{1,0:T(8,128)(2,1)S(1)} fusion(bf16[320,2048]{1,0:T(8,128)(2,1)} %all-gather.16.cloned.1.call-done, bf16[2048,1280]{1,0:T(8,128)(2,1)} %all-gather.20.cloned.1.call-done), kind=kOutput, calls=%fused_computation.3 | convolution fusion | flops 1678131200 | bytes 7372800 | tf_op jit(solution)/shard_map/dot_general | solution.py:110
  422.6 5.5 %fusion.2 = bf16[320,2048]{1,0:T(8,128)(2,1)} fusion(bf16[320,1280]{1,0:T(8,128)(2,1)S(1)} %fusion.21, bf16[1280,4096]{1,0:T(8,128)(2,1)} %constant_dynamic-update-slice_fusion, s32[]{:T(128)S(6)} %select_n.23), kind=kOutput, calls=%fused_computation.2 | convolution fusion | flops 1678376960 | bytes 7372804 | tf_op jit(solution)/shard_map/dot_general | solution.py:45
  428.1 24.9 %reduce-scatter.5.cloned.1.call-done = bf16[80,2048]{1,0:T(8,128)(2,1)} async-done(((bf16[320,2048]{1,0:T(8,128)(2,1)}), bf16[80,2048]{1,0:T(8,128)(2,1)}) %reduce-scatter.5.cloned.1.call-update) | async-done | bytes 327696 | tf_op jit(solution)/shard_map/reduce_scatter | solution.py:115
  454.2 1.9 fusion.38
  (70 shorter events, 23.4 us)
Async XLA Ops:
  6.5 33.1 %all-gather.10.cloned.1.call-start = ((), (), s32[]{:S(2)}) async-start(), calls=%async_computation.3 | async-start | bytes 1310720 | tf_op jit(solution)/shard_map/all_gather | solution.py:71
  7.3 51.5 %all-gather.8.cloned.1.call-start = ((), (), s32[]{:S(2)}) async-start(), calls=%async_computation.2 | async-start | bytes 1638400 | tf_op jit(solution)/shard_map/all_gather | solution.py:66
  11.0 77.4 %all-gather.12.cloned.1.call-start = ((), (), s32[]{:S(2)}) async-start(), calls=%async_computation.4 | async-start | bytes 1310720 | tf_op jit(solution)/shard_map/all_gather | solution.py:72
  11.8 105.4 %all-gather.14.cloned.1.call-start = ((), (), s32[]{:S(2)}) async-start(), calls=%async_computation.5 | async-start | bytes 1310720 | tf_op jit(solution)/shard_map/all_gather | solution.py:89
  12.3 133.6 %reduce-scatter.3.cloned.1.call-start = ((), (), s32[]{:S(2)}) async-start(), calls=%async_computation.6 | async-start | bytes 1638400 | tf_op jit(solution)/shard_map/reduce_scatter | solution.py:90
  58.8 29.6 %copy-start.6 = (bf16[320,2048]{1,0:T(8,128)(2,1)S(1)}, bf16[320,2048]{1,0:T(8,128)(2,1)}, u32[]{:S(2)}) copy-start(bf16[320,2048]{1,0:T(8,128)(2,1)} %all-gather.8.cloned.1.call-done) | copy-start | bytes 3932164
  97.8 22.3 %copy-start.3 = (bf16[2048]{0:T(1024)(128)(2,1)S(1)}, bf16[2048]{0:T(1024)(128)(2,1)}, u32[]{:S(2)}) copy-start(bf16[2048]{0:T(1024)(128)(2,1)} %param.21) | copy-start | bytes 12292
  97.8 22.3 %copy-start.4 = (bf16[2048]{0:T(1024)(128)(2,1)S(1)}, bf16[2048]{0:T(1024)(128)(2,1)}, u32[]{:S(2)}) copy-start(bf16[2048]{0:T(1024)(128)(2,1)} %param.22) | copy-start | bytes 12292
  97.8 49.3 %copy-start.1 = (bf16[80,2048]{1,0:T(8,128)(2,1)S(1)}, bf16[80,2048]{1,0:T(8,128)(2,1)}, u32[]{:S(2)}) copy-start(bf16[80,2048]{1,0:T(8,128)(2,1)} %param.14) | copy-start | bytes 983044
  120.0 219.4 %all-gather.16.cloned.1.call-start = ((), (), s32[]{:S(2)}) async-start(), calls=%async_computation.7 | async-start | bytes 1638400 | tf_op jit(solution)/shard_map/all_gather | solution.py:100
  149.3 1.6 copy-start
  149.3 125.9 %copy-start.2 = (bf16[2,3,5120]{2,0,1:T(2,128)(2,1)S(1)}, bf16[2,3,5120]{2,0,1:T(2,128)(2,1)}, u32[]{:S(2)}) copy-start(bf16[2,3,5120]{2,0,1:T(2,128)(2,1)} %param.25) | copy-start | bytes 184324
  149.4 190.1 %all-gather.18.cloned.1.call-start = ((), (), s32[]{:S(2)}) async-start(), calls=%async_computation.8 | async-start | bytes 6553600 | tf_op jit(solution)/shard_map/all_gather | solution.py:104
  150.1 266.1 %all-gather.20.cloned.1.call-start = ((), (), s32[]{:S(2)}) async-start(), calls=%async_computation.9 | async-start | bytes 6553600 | tf_op jit(solution)/shard_map/all_gather | solution.py:105
  150.9 302.2 %reduce-scatter.5.cloned.1.call-start = ((), (), s32[]{:S(2)}) async-start(), calls=%async_computation.10 | async-start | bytes 1638400 | tf_op jit(solution)/shard_map/reduce_scatter | solution.py:115
  150.9 33.7 %collective-permute-start = (bf16[1280,512]{1,0:T(8,128)(2,1)S(1)}, bf16[1280,512]{1,0:T(8,128)(2,1)S(1)}, u32[]{:S(2)}, u32[]{:S(2)}) collective-permute-start(bf16[1280,512]{1,0:T(8,128)(2,1)S(1)} %copy-done), channel_id=1, source_target_pairs={{0,4},{4,8},{8,12},{12,0},{1,5},{5,9},{9,13},{13,1},{2,6},{6,10},{... | collective-permute-start | bytes 3932168 | tf_op jit(solution)/shard_map/ppermute | solution.py:15
  184.6 61.5 %collective-permute-start.1 = (bf16[1280,512]{1,0:T(8,128)(2,1)S(1)}, bf16[1280,512]{1,0:T(8,128)(2,1)}, u32[]{:S(2)}, u32[]{:S(2)}) collective-permute-start(bf16[1280,512]{1,0:T(8,128)(2,1)S(1)} %collective-permute-done), channel_id=1, source_target_pairs={{0,4},{4,8},{8,12},{12,0},{1,5},{5,9},{9,13},{13,1},{2,6},{6,10},{... | collective-permute-start | bytes 3932168 | tf_op jit(solution)/shard_map/ppermute | solution.py:15
  246.1 77.8 %collective-permute-start.2 = (bf16[1280,512]{1,0:T(8,128)(2,1)}, bf16[1280,512]{1,0:T(8,128)(2,1)}, u32[]{:S(2)}, u32[]{:S(2)}) collective-permute-start(bf16[1280,512]{1,0:T(8,128)(2,1)} %collective-permute-done.1), channel_id=1, source_target_pairs={{0,4},{4,8},{8,12},{12,0},{1,5},{5,9},{9,13},{13,1},{2,6},{6,10},{... | collective-permute-start | bytes 3932168 | tf_op jit(solution)/shard_map/ppermute | solution.py:15
  422.6 5.5 %copy-start.5 = (bf16[2048]{0:T(1024)(128)(2,1)S(1)}, bf16[2048]{0:T(1024)(128)(2,1)}, u32[]{:S(2)}) copy-start(bf16[2048]{0:T(1024)(128)(2,1)} %param.27) | copy-start | bytes 12292
Sparse Core Ops, SparseCore 0:
  8.9 30.7 all-gather.9
  41.2 17.5 all-gather.7
  60.4 27.9 all-gather.11
  89.8 27.3 all-gather.13
  120.1 25.7 reduce-scatter.2
  149.5 18.1 all-gather.15
  169.3 147.2 all-gather.17
  318.2 98.0 all-gather.19
  428.2 24.7 reduce-scatter.4
